TPU v7x, 512 devices: a whole 4x8x8 slice. The times are simulated.
512 devices in a mesh: sp: 32 (over z, x), tp: 16 (over y, core).
Axes of the slice: x: 4, y: 8, z: 8, core: 2. Of those that a mesh axis runs over, the one named last changes fastest.
Arguments:
- latent: bfloat16 [16384, 2048], P('sp'), may hold values from -6 to 6
- context: bfloat16 [512, 2048], P('sp'), may hold values from -6 to 6
- condition: bfloat16 [2048], replicated, may hold values from -6 to 6
- context_condition: bfloat16 [2048], replicated, may hold values from -6 to 6
- shift_weight: bfloat16 [2048, 2048], P('sp', 'tp'), may hold values from -0.125 to 0.125
- scale_weight: bfloat16 [2048, 2048], P('sp', 'tp'), may hold values from -0.125 to 0.125
- mod_gate_weight: bfloat16 [2048, 2048], P('sp', 'tp'), may hold values from -0.5 to 0.5
- norm_gain: bfloat16 [2048], replicated, may hold values from 0.099609375 to 1.8984375
- query_weight: bfloat16 [2048, 2048], P(None, 'tp'), may hold values from -0.125 to 0.125
- key_weight: bfloat16 [2048, 2048], P(None, 'tp'), may hold values from -0.125 to 0.125
- value_weight: bfloat16 [2048, 2048], P(None, 'tp'), may hold values from -0.125 to 0.125
- gate_weight: bfloat16 [2048, 2048], P(None, 'tp'), may hold values from -0.125 to 0.125
- forward_decay: float32 [16], P('tp'), may hold values from 0 to 1, as said below
- backward_decay: float32 [16], P('tp'), may hold values from 0 to 1, as said below
- out_weight: bfloat16 [2048, 2048], P('tp'), may hold values from -0.125 to 0.125
Outputs:
- mixed: bfloat16 [16384, 2048], P('sp')
Inputs may be any that keep to these rules, and one draw needn't show every extreme that they name: `forward_decay`: each head's rate is positive. `backward_decay`: each head's rate is positive.
All inputs are finite; a program needn't handle non-finite values.
Results may differ from a plain program's by a relative error of at most 0.015.
Values may be sent and summed in bfloat16 or wider, within the bound.
No kernel may reach another device: no remote copies, remote signals or barrier semaphores. Data moves between devices by JAX's collectives and lax.ppermute only.
A program may use at most 64 MiB of HBM per device.

v0:
```python
import jax
import jax.numpy as jnp
from jax import lax
from jax.sharding import Mesh
from jax.sharding import PartitionSpec as P

HEAD_DIM = 128
GRID_W = 64
SP = ("sp_0", "sp_1")
EPS = 1e-06
THETA = 10000.0
CONTEXT_LIFT = 3.0
TOP_PRECISION = lax.Precision.HIGHEST


def sent_to_all(x, axis):
    copies = jnp.broadcast_to(x, (lax.axis_size(axis), *x.shape))
    return lax.all_to_all(copies, axis, split_axis=0, concat_axis=0, tiled=True)


def taken_together(x, axis):
    everything = sent_to_all(x, axis)
    return jnp.sum(everything, axis=0)


def in_one(arrays, axis):
    ravelled, at, finished = (jnp.concatenate([a.reshape(-1) for a in arrays]), 0, [])
    total = lax.psum(ravelled, axis)
    for a in arrays:
        finished.append(total[at : at + a.size].reshape(a.shape))
        at += a.size
    return tuple(finished)


def filled_with(x, identity):
    return jax.tree.map(
        lambda a, e: jnp.broadcast_to(jnp.asarray(e, a.dtype), a.shape), x, identity
    )


def all_in_one(x, axis):
    leaves = jax.tree.leaves(x)
    order = sorted(range(len(leaves)), key=lambda k: -leaves[k].size)
    width = (1, *leaves[order[0]].shape)[-1]
    lines = [
        jnp.pad(leaves[k].reshape(-1), (0, -leaves[k].size % width)).reshape(-1, width)
        for k in order
    ]
    both, at, found = (lax.all_gather(jnp.concatenate(lines), axis), 0, {})
    for k, line in zip(order, lines):
        slab = both[:, at : at + len(line)].reshape(len(both), -1)
        found[k] = slab[:, : leaves[k].size].reshape(-1, *leaves[k].shape)
        at += len(line)
    numbers = iter(range(len(leaves)))
    return jax.tree.map(lambda _: found[next(numbers)], x)


def prefix_by_axis(x, axes, combine, identity, reverse):
    before = start = filled_with(x, identity)
    total = x
    for axis in reversed(axes):
        length, mine = (lax.axis_size(axis), lax.axis_index(axis))
        pieces = all_in_one(total, axis)
        inside, total = (start, start)
        for k in reversed(range(length)) if reverse else range(length):
            passed = k > mine if reverse else k < mine
            total = combine(total, jax.tree.map(lambda part: part[k], pieces))
            inside = jax.tree.map(lambda new, old: jnp.where(passed, new, old), total, inside)
        before = combine(inside, before)
    return before


def laid_out(parts, dim):
    dims = list(parts.shape[1:])
    dims[dim] *= parts.shape[0]
    return jnp.moveaxis(parts, 0, dim).reshape(dims)


def collect(x, axis, dim):
    return laid_out(sent_to_all(x, axis), dim)


def modulated(token_rows, norm_gain, shifts, scales):
    values = token_rows.astype(jnp.float32)
    values = values * lax.rsqrt(jnp.mean(values * values, axis=-1, keepdims=True) + EPS)
    values = values * norm_gain.astype(jnp.float32)
    return (values * (1.0 + scales) + shifts).astype(jnp.bfloat16)


def rope_half(portion, positions):
    quarter = portion.shape[-1] // 2
    frequency = THETA ** (-jnp.arange(quarter, dtype=jnp.float32) / quarter)
    angles = positions[:, None, None] * frequency
    cosine = jnp.cos(angles)
    sine_table = jnp.sin(angles)
    leading = portion[..., :quarter]
    trailing = portion[..., quarter:]
    return jnp.concatenate(
        [leading * cosine - trailing * sine_table, leading * sine_table + trailing * cosine],
        axis=-1,
    )


def rotate(values, grid_row, grid_column):
    half_width = values.shape[-1] // 2
    return jnp.concatenate(
        [
            rope_half(values[..., :half_width], grid_row),
            rope_half(values[..., half_width:], grid_column),
        ],
        axis=-1,
    )


def combine(earlier, later):
    return (earlier[0] * later[0], later[0][:, None, None] * earlier[1] + later[1])


def local(
    latent,
    context,
    condition,
    context_condition,
    shift_weight,
    scale_weight,
    mod_gate_weight,
    norm_gain,
    query_weight,
    key_weight,
    value_weight,
    gate_weight,
    forward_decay,
    backward_decay,
    out_weight,
):
    sp_index = lax.axis_index(SP)
    tp_index = lax.axis_index("tp")
    sp_count = lax.axis_size(SP)
    tp_count = lax.axis_size("tp")
    tokens_here = latent.shape[0]
    local_rows = tokens_here // tp_count
    mod_rows = shift_weight.shape[0]
    activation = jax.nn.silu(jnp.stack([condition, context_condition]).astype(jnp.float32)).astype(
        jnp.bfloat16
    )
    own_part = lax.dynamic_slice_in_dim(activation, sp_index * mod_rows, mod_rows, 1)
    partial_value = jnp.stack(
        [
            jnp.dot(own_part, matrix, preferred_element_type=jnp.float32)
            for matrix in (shift_weight, scale_weight, mod_gate_weight)
        ]
    )
    summed = taken_together(partial_value, SP)
    modulation = lax.all_gather(summed, "tp", axis=2, tiled=True)
    hidden = modulated(latent, norm_gain, modulation[0, 0], modulation[1, 0])
    context_hidden = modulated(context, norm_gain, modulation[0, 1], modulation[1, 1])
    local_width = query_weight.shape[1]
    head_count = local_width // HEAD_DIM
    stacked = jnp.concatenate([query_weight, key_weight, value_weight, gate_weight], axis=1)
    projected = jnp.dot(hidden, stacked, preferred_element_type=jnp.float32).astype(jnp.bfloat16)
    queries = projected[:, :local_width]
    keys_out = projected[:, local_width : 2 * local_width]
    values_out = projected[:, 2 * local_width : 3 * local_width]
    out_gates = projected[:, 3 * local_width :]
    context_pairs = jnp.dot(
        context_hidden,
        stacked[:, local_width : 3 * local_width],
        preferred_element_type=jnp.float32,
    ).astype(jnp.bfloat16)

    def to_heads(values):
        return values.astype(jnp.float32).reshape(values.shape[0], head_count, HEAD_DIM)

    positions = sp_index * tokens_here + jnp.arange(tokens_here, dtype=jnp.int32)
    grid_row = (positions // GRID_W).astype(jnp.float32)
    grid_column = (positions % GRID_W).astype(jnp.float32)
    key_scale = HEAD_DIM ** (-0.5)
    query_heads = jnp.transpose(rotate(to_heads(queries), grid_row, grid_column), (1, 0, 2))
    key_heads = (
        jnp.transpose(rotate(to_heads(keys_out), grid_row, grid_column), (1, 0, 2)) * key_scale
    )
    value_heads = jnp.transpose(to_heads(values_out), (1, 0, 2))
    log_forward = -forward_decay
    log_backward = -backward_decay
    context_rows = context.shape[0]
    context_total = context_rows * sp_count
    context_index = (sp_index * context_rows + jnp.arange(context_rows, dtype=jnp.int32)).astype(
        jnp.float32
    )
    weight_forward = jnp.exp(log_forward[:, None] * (context_total - 1.0 - context_index)[None, :])
    weight_backward = jnp.exp(log_backward[:, None] * context_index[None, :])
    context_key_heads = to_heads(context_pairs[:, :local_width]) * (key_scale * CONTEXT_LIFT)
    context_value_heads = to_heads(context_pairs[:, local_width:])
    context_forward = jnp.einsum(
        "hc,chd,che->hde",
        weight_forward,
        context_key_heads,
        context_value_heads,
        precision=TOP_PRECISION,
    )
    context_backward = jnp.einsum(
        "hc,chd,che->hde",
        weight_backward,
        context_key_heads,
        context_value_heads,
        precision=TOP_PRECISION,
    )
    context_forward, context_backward = in_one((context_forward, context_backward), SP)
    offsets = jnp.arange(tokens_here, dtype=jnp.float32)
    distance = offsets[:, None] - offsets[None, :]
    mixing = jnp.where(
        distance >= 0, jnp.exp(log_forward[:, None, None] * jnp.maximum(distance, 0.0)), 0.0
    )
    mixing = mixing + jnp.where(
        distance <= 0, jnp.exp(log_backward[:, None, None] * jnp.maximum(-distance, 0.0)), 0.0
    )
    score_matrix = (
        jnp.einsum("htd,hsd->hts", query_heads, key_heads, precision=TOP_PRECISION) * mixing
    )
    local_out = jnp.einsum("hts,hse->hte", score_matrix, value_heads, precision=TOP_PRECISION)
    tail_forward = jnp.exp(log_forward[:, None] * (tokens_here - 1.0 - offsets)[None, :])
    head_backward = jnp.exp(log_backward[:, None] * offsets[None, :])
    own_forward = jnp.einsum(
        "ht,htd,hte->hde", tail_forward, key_heads, value_heads, precision=TOP_PRECISION
    )
    own_backward = jnp.einsum(
        "ht,htd,hte->hde", head_backward, key_heads, value_heads, precision=TOP_PRECISION
    )
    span_forward = jnp.exp(log_forward * tokens_here)
    span_backward = jnp.exp(log_backward * tokens_here)
    identity = (jnp.ones_like(span_forward), jnp.zeros_like(own_forward))
    before = prefix_by_axis((span_forward, own_forward), SP, combine, identity, False)
    after = prefix_by_axis((span_backward, own_backward), SP, combine, identity, True)
    device_start = (sp_index * tokens_here).astype(jnp.float32)
    device_rest = ((sp_count - 1 - sp_index) * tokens_here).astype(jnp.float32)
    incoming_forward = (
        before[1] + jnp.exp(log_forward * device_start)[:, None, None] * context_forward
    )
    incoming_backward = (
        after[1] + jnp.exp(log_backward * device_rest)[:, None, None] * context_backward
    )
    read_forward = jnp.exp(log_forward[:, None] * (offsets + 1.0)[None, :])[
        :, :, None
    ] * jnp.einsum("htd,hde->hte", query_heads, incoming_forward, precision=TOP_PRECISION)
    read_backward = jnp.exp(log_backward[:, None] * (tokens_here - offsets)[None, :])[
        :, :, None
    ] * jnp.einsum("htd,hde->hte", query_heads, incoming_backward, precision=TOP_PRECISION)
    retained = local_out + read_forward + read_backward
    retained = retained * lax.rsqrt(jnp.mean(retained * retained, axis=-1, keepdims=True) + EPS)
    merged = jnp.transpose(retained, (1, 0, 2)).reshape(tokens_here, local_width)
    heads_out = (jax.nn.silu(out_gates.astype(jnp.float32)) * merged).astype(jnp.bfloat16)
    projection = lax.psum_scatter(
        jnp.dot(heads_out, out_weight, preferred_element_type=jnp.float32),
        "tp",
        scatter_dimension=0,
        tiled=True,
    )
    own_latent = lax.dynamic_slice_in_dim(latent, tp_index * local_rows, local_rows, 0)
    finished = (own_latent.astype(jnp.float32) + modulation[2, 0] * projection).astype(jnp.bfloat16)
    return collect(finished, "tp", 0)


def solution(mesh):
    torus = Mesh(mesh.devices.reshape(8, 4, mesh.shape["tp"]), ("sp_0", "sp_1", "tp"))
    in_specs = (
        P(SP, None),
        P(SP, None),
        P(),
        P(),
        P(SP, "tp"),
        P(SP, "tp"),
        P(SP, "tp"),
        P(),
        P(None, "tp"),
        P(None, "tp"),
        P(None, "tp"),
        P(None, "tp"),
        P("tp"),
        P("tp"),
        P("tp", None),
    )
    out_specs = P(SP, None)
    return jax.shard_map(local, mesh=torus, in_specs=in_specs, out_specs=out_specs, check_vma=False)
```

profile of v0, /device:TPU:1, one launch (start us, length us, event | category | flops | bytes accessed | tf_op | source)
XLA Modules:
  0.0 352.9 jit_solution(17837896909596042663)
XLA Ops:
  6.5 0.8 stack.21
  7.4 0.7 stack.22
  8.1 0.9 convolution_bitcast_fusion.4
  9.0 0.9 convolution_bitcast_fusion.3
  9.9 0.9 convolution_bitcast_fusion.2
  10.9 0.7 broadcast_in_dim.10
  11.5 13.7 %all-to-all-start = ((f32[32,3,2,128]{3,2,1,0:T(2,128)}), f32[32,3,2,128]{3,2,1,0:T(2,128)S(1)}, u32[]{:S(2)}, u32[]{:S(2)}) async-start(f32[32,3,2,128]{3,2,1,0:T(2,128)} %broadcast_in_dim.10), calls=%async_computation | async-start | bytes 196608 | tf_op jit(solution)/shard_map/all_to_all | solution.py:18
  25.3 0.0 all-reduce.6.cloned.1.call-start
  27.0 1.0 fusion.45
  28.0 2.1 fusion
  30.0 0.7 convert_element_type.83
  30.7 3.6 %all-to-all-done = f32[32,3,2,128]{3,2,1,0:T(2,128)S(1)} async-done(((f32[32,3,2,128]{3,2,1,0:T(2,128)}), f32[32,3,2,128]{3,2,1,0:T(2,128)S(1)}, u32[]{:S(2)}, u32[]{:S(2)}) %all-to-all-start) | async-done | bytes 98336 | tf_op jit(solution)/shard_map/all_to_all | solution.py:18
  34.4 0.1 reduce_sum.36
  34.4 19.6 %all_gather.27 = f32[3,2,2048]{2,1,0:T(2,128)S(1)} all-gather(f32[3,2,128]{2,1,0:T(2,128)S(1)} %reduce_sum.36), channel_id=1, replica_groups=mesh['sp_0'=8,'sp_1'=4,'tp'=16] {'tp'}, dimensions={2}, use_global_device_ids=true | all-gather | bytes 52224 | tf_op jit(solution)/shard_map/all_gather | solution.py:154
  54.1 1.5 convolution_convert_fusion
  55.6 0.3 convolution_bitcast_fusion.1
  55.9 0.3 convolution_bitcast_fusion
  56.2 0.7 pad_maximum_fusion
  56.9 0.0 all-reduce.6.cloned.1.call-update
  56.9 0.0 reduce-scatter.2.cloned.1.call-start
  57.0 2.9 fusion.18
  59.9 0.1 fusion.53
  60.0 0.6 fusion.82
  60.6 0.3 fusion.40
  60.8 0.3 fusion.42
  61.1 9.4 %all-gather.4 = f32[4,129,128]{2,1,0:T(8,128)S(1)} all-gather(f32[1,129,128]{2,1,0:T(8,128)S(1)} %maximum_bitcast_fusion.4), channel_id=2, replica_groups=mesh['sp_0'=8,'sp_1'=4,'tp'=16] {'sp_1'}, dimensions={0}, use_global_device_ids=true | all-gather | bytes 330240 | tf_op jit(solution)/shard_map/all_gather | solution.py:49
  70.6 0.6 fusion.227
  74.4 9.7 %all-gather.6 = f32[4,129,128]{2,1,0:T(8,128)S(1)} all-gather(f32[1,129,128]{2,1,0:T(8,128)S(1)} %maximum_bitcast_fusion.6), channel_id=4, replica_groups=mesh['sp_0'=8,'sp_1'=4,'tp'=16] {'sp_1'}, dimensions={0}, use_global_device_ids=true | all-gather | bytes 330240 | tf_op jit(solution)/shard_map/all_gather | solution.py:49
  84.1 0.6 fusion.226
  89.2 2.0 fusion.233
  91.1 19.6 %all-gather.7 = f32[8,129,128]{2,1,0:T(8,128)S(1)} all-gather(f32[1,129,128]{2,1,0:T(8,128)S(1)} %maximum_bitcast_fusion.7), channel_id=5, replica_groups=mesh['sp_0'=8,'sp_1'=4,'tp'=16] {'sp_0'}, dimensions={0}, use_global_device_ids=true | all-gather | bytes 594432 | tf_op jit(solution)/shard_map/all_gather | solution.py:49
  110.7 0.7 fusion.224
  111.4 1.9 fusion.234
  113.3 20.3 %all-gather.5 = f32[8,129,128]{2,1,0:T(8,128)S(1)} all-gather(f32[1,129,128]{2,1,0:T(8,128)S(1)} %maximum_bitcast_fusion.5), channel_id=3, replica_groups=mesh['sp_0'=8,'sp_1'=4,'tp'=16] {'sp_0'}, dimensions={0}, use_global_device_ids=true | all-gather | bytes 594432 | tf_op jit(solution)/shard_map/all_gather | solution.py:49
  133.7 0.7 fusion.225
  135.6 1.5 convolution_multiply_fusion
  137.2 0.7 fusion.62
  137.9 61.9 %all-reduce.6.cloned.1.call-done = f32[32768]{0:T(1024)} async-done(((f32[32768]{0:T(1024)}), f32[32768]{0:T(1024)}) %all-reduce.6.cloned.1.call-update) | async-done | bytes 131088 | tf_op jit(solution)/shard_map/psum | solution.py:28
  199.9 8.0 %fusion.24 = f32[512,128]{0,1:T(8,128)S(1)} fusion(f32[512,128]{0,1:T(8,128)S(1)} %fusion.62, f32[512]{0:T(512)S(1)} %multiply_exponential_fusion.1, f32[32768]{0:T(1024)} %all-reduce.6.cloned.1.call-done, f32[8,129,128]{2,1,0:T(8,128)} %copy-done.3, f32[4,129,128]{2,1,0:T(8,128)S(1)} %all-gather.4, f32[512,1,32]{0,2,1:T(8,128)} %copy-done.5, ...), kind=kOutput, calls=%fused_computation.26 | convolution fusion | flops 101695488 | bytes 1847816 | tf_op jit(solution)/shard_map/htd,hde->hte/dot_general | solution.py:244
  207.9 8.0 %multiply_reduce_fusion = (f32[512]{0:T(512)S(1)}, f32[512,128]{0,1:T(8,128)S(1)}) fusion(f32[512,128]{0,1:T(8,128)S(1)} %fusion.24, f32[32768]{0:T(1024)} %all-reduce.6.cloned.1.call-done, f32[8,129,128]{2,1,0:T(8,128)} %copy-done.2, f32[4,129,128]{2,1,0:T(8,128)S(1)} %all-gather.6, f32[]{:T(128)} %bitcast.75, f32[]{:T(128)} %bitcast.76, f32[]{:T(128)} %bitcast.77, ...), kind=kOutput, calls=%fused_computation.53 | convolution fusion | flops 101826048 | bytes 1849864 | tf_op jit(solution)/shard_map/htd,hde->hte/dot_general | solution.py:247
  215.9 0.0 copy-done
  215.9 3.6 %fusion.50 = f32[512,2048]{1,0:T(8,128)} fusion(bf16[128,2048]{1,0:T(8,128)(2,1)S(1)} %copy-done, f32[512,128]{0,1:T(8,128)S(1)} %get-tuple-element.53, bf16[512,512]{0,1:T(8,128)(2,1)} %copy-done.4, f32[512]{0:T(512)S(1)} %add_rsqrt_fusion), kind=kOutput, calls=%fused_computation.66 | convolution fusion | flops 268959744 | bytes 5113856 | tf_op jit(solution)/shard_map/dot_general | solution.py:253
  219.5 0.0 reduce-scatter.2.cloned.1.call-update
  219.5 66.3 %reduce-scatter.2.cloned.1.call-done = f32[32,2048]{1,0:T(8,128)} async-done(((f32[512,2048]{1,0:T(8,128)}), f32[32,2048]{1,0:T(8,128)}) %reduce-scatter.2.cloned.1.call-update) | async-done | bytes 262160 | tf_op jit(solution)/shard_map/reduce_scatter | solution.py:252
  285.8 1.0 add_convert_fusion
  286.8 0.2 broadcast_in_dim.12
  287.1 57.7 %all_to_all.10 = bf16[16,32,2048]{2,1,0:T(8,128)(2,1)S(1)} all-to-all(bf16[16,32,2048]{2,1,0:T(8,128)(2,1)S(1)} %broadcast_in_dim.12), channel_id=1, replica_groups=mesh['sp_0'=8,'sp_1'=4,'tp'=16] {'tp'}, dimensions={0} | all-to-all | bytes 4194304 | tf_op jit(solution)/shard_map/all_to_all | solution.py:18
  344.8 1.3 copy.34
  (42 shorter events, 0.3 us)
Async XLA Ops:
  6.5 209.4 %copy-start = (bf16[128,2048]{1,0:T(8,128)(2,1)S(1)}, bf16[128,2048]{1,0:T(8,128)(2,1)}, u32[]{:S(2)}) copy-start(bf16[128,2048]{1,0:T(8,128)(2,1)} %param.29) | copy-start | bytes 1572868
  6.5 50.4 %copy-start.1 = (bf16[512,2048]{1,0:T(8,128)(2,1)S(1)}, bf16[512,2048]{1,0:T(8,128)(2,1)}, u32[]{:S(2)}) copy-start(bf16[512,2048]{1,0:T(8,128)(2,1)} %param.15) | copy-start | bytes 6291460
  6.5 50.4 %copy-start.8 = (bf16[2048,128]{1,0:T(8,128)(2,1)S(1)}, bf16[2048,128]{1,0:T(8,128)(2,1)}, u32[]{:S(2)}) copy-start(bf16[2048,128]{1,0:T(8,128)(2,1)} %param.25) | copy-start | bytes 1572868
  11.5 22.8 %all-to-all-start = ((f32[32,3,2,128]{3,2,1,0:T(2,128)}), f32[32,3,2,128]{3,2,1,0:T(2,128)S(1)}, u32[]{:S(2)}, u32[]{:S(2)}) async-start(f32[32,3,2,128]{3,2,1,0:T(2,128)} %broadcast_in_dim.10), calls=%async_computation | async-start | bytes 196608 | tf_op jit(solution)/shard_map/all_to_all | solution.py:18
  25.3 174.6 %all-reduce.6.cloned.1.call-start = ((), (), s32[]{:S(2)}) async-start(), calls=%async_computation.3 | async-start | bytes 262144 | tf_op jit(solution)/shard_map/psum | solution.py:28
  56.9 228.9 %reduce-scatter.2.cloned.1.call-start = ((), (), s32[]{:S(2)}) async-start(), calls=%async_computation.4 | async-start | bytes 4456448 | tf_op jit(solution)/shard_map/reduce_scatter | solution.py:252
  59.9 77.3 %copy-start.4 = (bf16[512,512]{0,1:T(8,128)(2,1)}, bf16[512,512]{0,1:T(8,128)(2,1)S(1)}, u32[]{:S(2)}) copy-start(bf16[512,512]{0,1:T(8,128)(2,1)S(1)} %fusion.18) | copy-start | bytes 1572868
  60.5 76.6 %copy-start.5 = (f32[512,1,32]{0,2,1:T(8,128)}, f32[512,1,32]{0,2,1:T(8,128)S(1)}, u32[]{:S(2)}) copy-start(f32[512,1,32]{0,2,1:T(8,128)S(1)} %get-tuple-element.25) | copy-start | bytes 196612
  60.5 76.6 %copy-start.6 = (f32[512,1,32]{0,2,1:T(8,128)}, f32[512,1,32]{0,2,1:T(8,128)S(1)}, u32[]{:S(2)}) copy-start(f32[512,1,32]{0,2,1:T(8,128)S(1)} %get-tuple-element.26) | copy-start | bytes 196612
  60.6 76.6 %copy-start.7 = (f32[512,1,32]{0,2,1:T(8,128)}, f32[512,1,32]{0,2,1:T(8,128)S(1)}, u32[]{:S(2)}) copy-start(f32[512,1,32]{0,2,1:T(8,128)S(1)} %get-tuple-element.27) | copy-start | bytes 196612
  110.7 24.9 %copy-start.2 = (f32[8,129,128]{2,1,0:T(8,128)}, f32[8,129,128]{2,1,0:T(8,128)S(1)}, u32[]{:S(2)}) copy-start(f32[8,129,128]{2,1,0:T(8,128)S(1)} %all-gather.7) | copy-start | bytes 1585156
  133.7 2.0 copy-start.3
Sparse Core Ops, SparseCore 0:
  57.0 142.7 all-reduce.5
  219.6 66.1 reduce-scatter.1
where the time goes:
time: 354 us; the launch traced here: 353 us
  blocking collectives  136 us (38%)
  waiting for transfers between devices  132 us (37%)
  matrix products  30.2 us (9%)
  between operations  24.2 us (7%)
  starting transfers between devices  13.8 us (4%)
  other arithmetic  10.1 us (3%)
  local copies, waits for them, and re-layouts  6.43 us (2%)
    reduce_scatter x1, waiting for transfers between devices, local(): lax.psum_scatter(jnp.dot(heads_out, out_weight, preferred_element_type=jn...  66.3 us
    psum x1, waiting for transfers between devices, in_one(): total = lax.psum(ravelled, axis)  61.9 us
    all_gather x4, blocking collectives, all_in_one(): both, at, found = (lax.all_gather(jnp.concatenate(lines), axis), 0, {})  59 us
    all_to_all x1, blocking collectives, sent_to_all(): return lax.all_to_all(copies, axis, split_axis=0, concat_axis=0, tiled=True)  57.7 us
    all_gather x1, blocking collectives, local(): modulation = lax.all_gather(summed, 'tp', axis=2, tiled=True)  19.6 us
    all_to_all x1, starting transfers between devices, sent_to_all(): return lax.all_to_all(copies, axis, split_axis=0, concat_axis=0, tiled=True)  13.7 us
    dot_general x1, matrix products, local(): jnp.einsum('htd,hde->hte', query_heads, incoming_forward, precision=TOP_P...  8.03 us
    dot_general x1, matrix products, local(): jnp.einsum('htd,hde->hte', query_heads, incoming_backward, precision=TOP_...  7.98 us
  transfers between devices with their start and end apart: 3, of which 3 were waited for; matrix products, arithmetic and copies ran while one was open for 5% of the time, Pallas kernels for 0%

commit v1 on v0

--- a/solution.py
+++ b/solution.py
@@ -11,6 +11,24 @@
 THETA = 10000.0
 CONTEXT_LIFT = 3.0
 TOP_PRECISION = lax.Precision.HIGHEST
+
+
+def gather_around(shard, axis, dim):
+    ways, here, step = (lax.axis_size(axis), lax.axis_index(axis), shard.shape[dim])
+    lengths = [n * ways if d == dim else n for d, n in enumerate(shard.shape)]
+    full = lax.dynamic_update_slice_in_dim(
+        jnp.zeros(lengths, shard.dtype), shard, here * step, axis=dim
+    )
+    going_up = going_down = shard
+    for far in range(1, ways // 2 + 1):
+        going_up = lax.ppermute(going_up, axis, [(d, (d + 1) % ways) for d in range(ways)])
+        full = lax.dynamic_update_slice_in_dim(full, going_up, (here - far) % ways * step, axis=dim)
+        if 2 * far < ways:
+            going_down = lax.ppermute(going_down, axis, [(d, (d - 1) % ways) for d in range(ways)])
+            full = lax.dynamic_update_slice_in_dim(
+                full, going_down, (here + far) % ways * step, axis=dim
+            )
+    return full
 
 
 def sent_to_all(x, axis):
@@ -151,7 +169,7 @@
         ]
     )
     summed = taken_together(partial_value, SP)
-    modulation = lax.all_gather(summed, "tp", axis=2, tiled=True)
+    modulation = gather_around(summed, "tp", 2)
     hidden = modulated(latent, norm_gain, modulation[0, 0], modulation[1, 0])
     context_hidden = modulated(context, norm_gain, modulation[0, 1], modulation[1, 1])
     local_width = query_weight.shape[1]

time: 354 us -> 373 us (1.054)
  starting transfers between devices: 13.8 us -> 36.2 us
  blocking collectives: 136 us -> 117 us
  waiting for transfers between devices: 132 us -> 148 us
    ppermute x0 -> x15, starting transfers between devices: none -> 22.4 us  [the longest x7 13.5 us: gather_around(): lax.ppermute(going_down, axis, [(d, (d - 1) % ways) for d in range(ways)])]
    all_gather x1 -> x0, blocking collectives: 19.6 us -> none  [local(): modulation = lax.all_gather(summed, 'tp', axis=2, tiled=True)]
    ppermute x0 -> x15, waiting for transfers between devices: none -> 9.76 us  [the longest x8 8.34 us: gather_around(): lax.ppermute(going_up, axis, [(d, (d + 1) % ways) for d in range(ways)])]
    psum x1, waiting for transfers between devices: 61.9 us -> 68 us  [in_one(): total = lax.psum(ravelled, axis)]
  transfers between devices with their start and end apart: 3 -> 18, of which waited for: 3 -> 17; matrix products, arithmetic and copies ran while one was open for 5% -> 5% of each run, Pallas kernels for 0% -> 0%
where the time goes in v1:
time: 373 us; the launch traced here: 372 us
  waiting for transfers between devices  148 us (40%)
  blocking collectives  117 us (31%)
  starting transfers between devices  36.2 us (10%)
  matrix products  30 us (8%)
  between operations  24.2 us (6%)
  other arithmetic  10.1 us (3%)
  local copies, waits for them, and re-layouts  6.61 us (2%)
    psum x1, waiting for transfers between devices, in_one(): total = lax.psum(ravelled, axis)  68 us
    reduce_scatter x1, waiting for transfers between devices, local(): lax.psum_scatter(jnp.dot(heads_out, out_weight, preferred_element_type=jn...  66.3 us
    all_gather x4, blocking collectives, all_in_one(): both, at, found = (lax.all_gather(jnp.concatenate(lines), axis), 0, {})  59.7 us
    all_to_all x1, blocking collectives, sent_to_all(): return lax.all_to_all(copies, axis, split_axis=0, concat_axis=0, tiled=True)  57.4 us
    all_to_all x1, starting transfers between devices, sent_to_all(): return lax.all_to_all(copies, axis, split_axis=0, concat_axis=0, tiled=True)  13.7 us
    ppermute x7, starting transfers between devices, gather_around(): lax.ppermute(going_down, axis, [(d, (d - 1) % ways) for d in range(ways)])  13.5 us
    ppermute x8, starting transfers between devices, gather_around(): lax.ppermute(going_up, axis, [(d, (d + 1) % ways) for d in range(ways)])  8.94 us
    ppermute x8, waiting for transfers between devices, gather_around(): lax.ppermute(going_up, axis, [(d, (d + 1) % ways) for d in range(ways)])  8.34 us
  transfers between devices with their start and end apart: 18, of which 17 were waited for; matrix products, arithmetic and copies ran while one was open for 5% of the time, Pallas kernels for 0%

profile of v1, /device:TPU:1, one launch (start us, length us, event | category | flops | bytes accessed | tf_op | source)
XLA Modules:
  0.0 371.8 jit_solution(7758503060309841547)
XLA Ops:
  6.5 0.8 stack.21
  7.4 0.7 stack.22
  8.1 0.9 convolution_bitcast_fusion.4
  9.0 0.9 convolution_bitcast_fusion.3
  9.9 0.9 convolution_bitcast_fusion.2
  10.9 0.7 broadcast_in_dim.13
  11.5 13.7 %all-to-all-start = ((f32[32,3,2,128]{3,2,1,0:T(2,128)}), f32[32,3,2,128]{3,2,1,0:T(2,128)S(1)}, u32[]{:S(2)}, u32[]{:S(2)}) async-start(f32[32,3,2,128]{3,2,1,0:T(2,128)} %broadcast_in_dim.13), calls=%async_computation | async-start | bytes 196608 | tf_op jit(solution)/shard_map/all_to_all | solution.py:36
  27.2 1.0 fusion.45
  28.2 2.1 fusion
  30.3 0.7 convert_element_type.83
  31.0 3.4 all-to-all-done
  34.4 3.3 collective-permute-start
  37.7 0.7 collective-permute-done
  38.4 2.3 collective-permute-start.2
  40.8 0.7 collective-permute-done.2
  41.5 2.3 collective-permute-start.4
  44.0 1.0 collective-permute-start.5
  45.0 0.6 collective-permute-done.4
  45.6 1.1 collective-permute-start.6
  47.1 2.2 collective-permute-start.7
  49.3 0.6 collective-permute-done.6
  50.1 3.4 collective-permute-start.9
  53.5 0.6 collective-permute-done.8
  54.3 3.4 collective-permute-start.11
  58.5 3.4 collective-permute-start.13
  62.8 4.0 %collective-permute-done.14 = f32[3,2,128]{2,1,0:T(2,128)S(1)} collective-permute-done((f32[3,2,128]{2,1,0:T(2,128)S(1)}, f32[3,2,128]{2,1,0:T(2,128)S(1)}, u32[]{:S(2)}, u32[]{:S(2)}) %collective-permute-start.14) | collective-permute-done | bytes 3104 | tf_op jit(solution)/shard_map/ppermute | solution.py:24
  66.8 1.5 convolution_convert_fusion
  69.0 0.7 pad_maximum_fusion
  69.8 2.9 fusion.18
  73.9 9.4 %all-gather.4 = f32[4,129,128]{2,1,0:T(8,128)S(1)} all-gather(f32[1,129,128]{2,1,0:T(8,128)S(1)} %maximum_bitcast_fusion.4), channel_id=2, replica_groups=mesh['sp_0'=8,'sp_1'=4,'tp'=16] {'sp_1'}, dimensions={0}, use_global_device_ids=true | all-gather | bytes 330240 | tf_op jit(solution)/shard_map/all_gather | solution.py:67
  83.3 0.6 fusion.227
  87.2 9.8 %all-gather.6 = f32[4,129,128]{2,1,0:T(8,128)S(1)} all-gather(f32[1,129,128]{2,1,0:T(8,128)S(1)} %maximum_bitcast_fusion.6), channel_id=4, replica_groups=mesh['sp_0'=8,'sp_1'=4,'tp'=16] {'sp_1'}, dimensions={0}, use_global_device_ids=true | all-gather | bytes 330240 | tf_op jit(solution)/shard_map/all_gather | solution.py:67
  101.8 1.8 fusion.233
  103.6 19.9 %all-gather.7 = f32[8,129,128]{2,1,0:T(8,128)S(1)} all-gather(f32[1,129,128]{2,1,0:T(8,128)S(1)} %maximum_bitcast_fusion.7), channel_id=5, replica_groups=mesh['sp_0'=8,'sp_1'=4,'tp'=16] {'sp_0'}, dimensions={0}, use_global_device_ids=true | all-gather | bytes 594432 | tf_op jit(solution)/shard_map/all_gather | solution.py:67
  123.5 0.7 fusion.224
  124.2 2.0 fusion.234
  126.2 20.6 %all-gather.5 = f32[8,129,128]{2,1,0:T(8,128)S(1)} all-gather(f32[1,129,128]{2,1,0:T(8,128)S(1)} %maximum_bitcast_fusion.5), channel_id=3, replica_groups=mesh['sp_0'=8,'sp_1'=4,'tp'=16] {'sp_0'}, dimensions={0}, use_global_device_ids=true | all-gather | bytes 594432 | tf_op jit(solution)/shard_map/all_gather | solution.py:67
  146.8 0.7 fusion.225
  148.8 1.5 convolution_multiply_fusion
  150.4 0.7 fusion.62
  151.1 68.0 %all-reduce.6.cloned.1.call-done = f32[32768]{0:T(1024)} async-done(((f32[32768]{0:T(1024)}), f32[32768]{0:T(1024)}) %all-reduce.6.cloned.1.call-update) | async-done | bytes 131088 | tf_op jit(solution)/shard_map/psum | solution.py:46
  219.1 7.9 %fusion.24 = f32[512,128]{0,1:T(8,128)S(1)} fusion(f32[512,128]{0,1:T(8,128)S(1)} %fusion.62, f32[512]{0:T(512)S(1)} %multiply_exponential_fusion.1, f32[32768]{0:T(1024)} %all-reduce.6.cloned.1.call-done, f32[8,129,128]{2,1,0:T(8,128)} %copy-done.3, f32[4,129,128]{2,1,0:T(8,128)S(1)} %all-gather.4, f32[512,1,32]{0,2,1:T(8,128)} %copy-done.5, ...), kind=kOutput, calls=%fused_computation.26 | convolution fusion | flops 101695488 | bytes 1847816 | tf_op jit(solution)/shard_map/htd,hde->hte/dot_general | solution.py:262
  227.1 7.9 %multiply_reduce_fusion = (f32[512]{0:T(512)S(1)}, f32[512,128]{0,1:T(8,128)S(1)}) fusion(f32[512,128]{0,1:T(8,128)S(1)} %fusion.24, f32[32768]{0:T(1024)} %all-reduce.6.cloned.1.call-done, f32[8,129,128]{2,1,0:T(8,128)} %copy-done.2, f32[4,129,128]{2,1,0:T(8,128)S(1)} %all-gather.6, f32[]{:T(128)} %bitcast.75, f32[]{:T(128)} %bitcast.76, f32[]{:T(128)} %bitcast.77, ...), kind=kOutput, calls=%fused_computation.53 | convolution fusion | flops 101826048 | bytes 1849864 | tf_op jit(solution)/shard_map/htd,hde->hte/dot_general | solution.py:265
  235.0 3.6 fusion.50
  238.6 66.3 %reduce-scatter.2.cloned.1.call-done = f32[32,2048]{1,0:T(8,128)} async-done(((f32[512,2048]{1,0:T(8,128)}), f32[32,2048]{1,0:T(8,128)}) %reduce-scatter.2.cloned.1.call-update) | async-done | bytes 262160 | tf_op jit(solution)/shard_map/reduce_scatter | solution.py:270
  304.9 1.0 add_convert_fusion
  306.2 57.4 %all_to_all.10 = bf16[16,32,2048]{2,1,0:T(8,128)(2,1)S(1)} all-to-all(bf16[16,32,2048]{2,1,0:T(8,128)(2,1)S(1)} %broadcast_in_dim.15), channel_id=1, replica_groups=mesh['sp_0'=8,'sp_1'=4,'tp'=16] {'tp'}, dimensions={0} | all-to-all | bytes 4194304 | tf_op jit(solution)/shard_map/all_to_all | solution.py:36
  363.6 1.3 copy.50
  (88 shorter events, 5.9 us)
Async XLA Ops:
  6.5 228.4 %copy-start = (bf16[128,2048]{1,0:T(8,128)(2,1)S(1)}, bf16[128,2048]{1,0:T(8,128)(2,1)}, u32[]{:S(2)}) copy-start(bf16[128,2048]{1,0:T(8,128)(2,1)} %param.29) | copy-start | bytes 1572868
  6.5 63.2 %copy-start.1 = (bf16[512,2048]{1,0:T(8,128)(2,1)S(1)}, bf16[512,2048]{1,0:T(8,128)(2,1)}, u32[]{:S(2)}) copy-start(bf16[512,2048]{1,0:T(8,128)(2,1)} %param.15) | copy-start | bytes 6291460
  6.5 63.2 %copy-start.8 = (bf16[2048,128]{1,0:T(8,128)(2,1)S(1)}, bf16[2048,128]{1,0:T(8,128)(2,1)}, u32[]{:S(2)}) copy-start(bf16[2048,128]{1,0:T(8,128)(2,1)} %param.25) | copy-start | bytes 1572868
  11.5 22.8 %all-to-all-start = ((f32[32,3,2,128]{3,2,1,0:T(2,128)}), f32[32,3,2,128]{3,2,1,0:T(2,128)S(1)}, u32[]{:S(2)}, u32[]{:S(2)}) async-start(f32[32,3,2,128]{3,2,1,0:T(2,128)} %broadcast_in_dim.13), calls=%async_computation | async-start | bytes 196608 | tf_op jit(solution)/shard_map/all_to_all | solution.py:36
  25.3 193.9 %all-reduce.6.cloned.1.call-start = ((), (), s32[]{:S(2)}) async-start(), calls=%async_computation.3 | async-start | bytes 262144 | tf_op jit(solution)/shard_map/psum | solution.py:46
  34.4 4.0 %collective-permute-start = (f32[3,2,128]{2,1,0:T(2,128)S(1)}, f32[3,2,128]{2,1,0:T(2,128)S(1)}, u32[]{:S(2)}, u32[]{:S(2)}) collective-permute-start(f32[3,2,128]{2,1,0:T(2,128)S(1)} %reduce_sum.36), channel_id=1, source_target_pairs={{0,1},{1,2},{2,3},{3,4},{4,5},{5,6},{6,7},{7,8},{8,9},{9,10},{10,1... | collective-permute-start | bytes 9224 | tf_op jit(solution)/shard_map/ppermute | solution.py:24
  37.7 3.0 collective-permute-start.1
  38.4 3.0 collective-permute-start.2
  40.7 3.3 collective-permute-start.3
  41.5 4.2 %collective-permute-start.4 = (f32[3,2,128]{2,1,0:T(2,128)S(1)}, f32[3,2,128]{2,1,0:T(2,128)S(1)}, u32[]{:S(2)}, u32[]{:S(2)}) collective-permute-start(f32[3,2,128]{2,1,0:T(2,128)S(1)} %collective-permute-done.2), channel_id=1, source_target_pairs={{0,1},{1,2},{2,3},{3,4},{4,5},{5,6},{6,7},{7,8},{8,9},{9,10},{10,1... | collective-permute-start | bytes 9224 | tf_op jit(solution)/shard_map/ppermute | solution.py:24
  44.0 3.0 collective-permute-start.5
  45.6 4.2 %collective-permute-start.6 = (f32[3,2,128]{2,1,0:T(2,128)S(1)}, f32[3,2,128]{2,1,0:T(2,128)S(1)}, u32[]{:S(2)}, u32[]{:S(2)}) collective-permute-start(f32[3,2,128]{2,1,0:T(2,128)S(1)} %collective-permute-done.4), channel_id=1, source_target_pairs={{0,1},{1,2},{2,3},{3,4},{4,5},{5,6},{6,7},{7,8},{8,9},{9,10},{10,1... | collective-permute-start | bytes 9224 | tf_op jit(solution)/shard_map/ppermute | solution.py:24
  47.1 3.0 collective-permute-start.7
  49.9 4.2 %collective-permute-start.8 = (f32[3,2,128]{2,1,0:T(2,128)S(1)}, f32[3,2,128]{2,1,0:T(2,128)S(1)}, u32[]{:S(2)}, u32[]{:S(2)}) collective-permute-start(f32[3,2,128]{2,1,0:T(2,128)S(1)} %collective-permute-done.6), channel_id=1, source_target_pairs={{0,1},{1,2},{2,3},{3,4},{4,5},{5,6},{6,7},{7,8},{8,9},{9,10},{10,1... | collective-permute-start | bytes 9224 | tf_op jit(solution)/shard_map/ppermute | solution.py:24
  50.1 4.2 %collective-permute-start.9 = (f32[3,2,128]{2,1,0:T(2,128)S(1)}, f32[3,2,128]{2,1,0:T(2,128)S(1)}, u32[]{:S(2)}, u32[]{:S(2)}) collective-permute-start(f32[3,2,128]{2,1,0:T(2,128)S(1)} %collective-permute-done.7), channel_id=1, source_target_pairs={{0,15},{1,0},{2,1},{3,2},{4,3},{5,4},{6,5},{7,6},{8,7},{9,8},{10,9... | collective-permute-start | bytes 9224 | tf_op jit(solution)/shard_map/ppermute | solution.py:27
  54.1 4.2 %collective-permute-start.10 = (f32[3,2,128]{2,1,0:T(2,128)S(1)}, f32[3,2,128]{2,1,0:T(2,128)S(1)}, u32[]{:S(2)}, u32[]{:S(2)}) collective-permute-start(f32[3,2,128]{2,1,0:T(2,128)S(1)} %collective-permute-done.8), channel_id=1, source_target_pairs={{0,1},{1,2},{2,3},{3,4},{4,5},{5,6},{6,7},{7,8},{8,9},{9,10},{10,1... | collective-permute-start | bytes 9224 | tf_op jit(solution)/shard_map/ppermute | solution.py:24
  54.3 4.2 %collective-permute-start.11 = (f32[3,2,128]{2,1,0:T(2,128)S(1)}, f32[3,2,128]{2,1,0:T(2,128)S(1)}, u32[]{:S(2)}, u32[]{:S(2)}) collective-permute-start(f32[3,2,128]{2,1,0:T(2,128)S(1)} %collective-permute-done.9), channel_id=1, source_target_pairs={{0,15},{1,0},{2,1},{3,2},{4,3},{5,4},{6,5},{7,6},{8,7},{9,8},{10,9... | collective-permute-start | bytes 9224 | tf_op jit(solution)/shard_map/ppermute | solution.py:27
  58.3 4.2 %collective-permute-start.12 = (f32[3,2,128]{2,1,0:T(2,128)S(1)}, f32[3,2,128]{2,1,0:T(2,128)S(1)}, u32[]{:S(2)}, u32[]{:S(2)}) collective-permute-start(f32[3,2,128]{2,1,0:T(2,128)S(1)} %collective-permute-done.10), channel_id=1, source_target_pairs={{0,1},{1,2},{2,3},{3,4},{4,5},{5,6},{6,7},{7,8},{8,9},{9,10},{10,1... | collective-permute-start | bytes 9224 | tf_op jit(solution)/shard_map/ppermute | solution.py:24
  58.5 4.2 %collective-permute-start.13 = (f32[3,2,128]{2,1,0:T(2,128)S(1)}, f32[3,2,128]{2,1,0:T(2,128)S(1)}, u32[]{:S(2)}, u32[]{:S(2)}) collective-permute-start(f32[3,2,128]{2,1,0:T(2,128)S(1)} %collective-permute-done.11), channel_id=1, source_target_pairs={{0,15},{1,0},{2,1},{3,2},{4,3},{5,4},{6,5},{7,6},{8,7},{9,8},{10,9... | collective-permute-start | bytes 9224 | tf_op jit(solution)/shard_map/ppermute | solution.py:27
  62.6 4.2 %collective-permute-start.14 = (f32[3,2,128]{2,1,0:T(2,128)S(1)}, f32[3,2,128]{2,1,0:T(2,128)S(1)}, u32[]{:S(2)}, u32[]{:S(2)}) collective-permute-start(f32[3,2,128]{2,1,0:T(2,128)S(1)} %collective-permute-done.12), channel_id=1, source_target_pairs={{0,1},{1,2},{2,3},{3,4},{4,5},{5,6},{6,7},{7,8},{8,9},{9,10},{10,1... | collective-permute-start | bytes 9224 | tf_op jit(solution)/shard_map/ppermute | solution.py:24
  69.7 235.2 %reduce-scatter.2.cloned.1.call-start = ((), (), s32[]{:S(2)}) async-start(), calls=%async_computation.4 | async-start | bytes 4456448 | tf_op jit(solution)/shard_map/reduce_scatter | solution.py:270
  72.7 77.7 %copy-start.4 = (bf16[512,512]{0,1:T(8,128)(2,1)}, bf16[512,512]{0,1:T(8,128)(2,1)S(1)}, u32[]{:S(2)}) copy-start(bf16[512,512]{0,1:T(8,128)(2,1)S(1)} %fusion.18) | copy-start | bytes 1572868
  73.3 77.1 %copy-start.5 = (f32[512,1,32]{0,2,1:T(8,128)}, f32[512,1,32]{0,2,1:T(8,128)S(1)}, u32[]{:S(2)}) copy-start(f32[512,1,32]{0,2,1:T(8,128)S(1)} %get-tuple-element.25) | copy-start | bytes 196612
  73.3 77.1 %copy-start.6 = (f32[512,1,32]{0,2,1:T(8,128)}, f32[512,1,32]{0,2,1:T(8,128)S(1)}, u32[]{:S(2)}) copy-start(f32[512,1,32]{0,2,1:T(8,128)S(1)} %get-tuple-element.26) | copy-start | bytes 196612
  73.3 77.1 %copy-start.7 = (f32[512,1,32]{0,2,1:T(8,128)}, f32[512,1,32]{0,2,1:T(8,128)S(1)}, u32[]{:S(2)}) copy-start(f32[512,1,32]{0,2,1:T(8,128)S(1)} %get-tuple-element.27) | copy-start | bytes 196612
  123.5 25.3 %copy-start.2 = (f32[8,129,128]{2,1,0:T(8,128)}, f32[8,129,128]{2,1,0:T(8,128)S(1)}, u32[]{:S(2)}) copy-start(f32[8,129,128]{2,1,0:T(8,128)S(1)} %all-gather.7) | copy-start | bytes 1585156
  146.8 2.0 copy-start.3
Sparse Core Ops, SparseCore 0:
  69.8 149.2 all-reduce.5
  238.7 66.1 reduce-scatter.1
